TPU v7x, 32 devices: a whole 2x2x4 slice. The times are simulated.
32 devices in a mesh: grp: 2 (over x), sp: 4 (over y, core), tp: 4 (over z).
Axes of the slice: x: 2, y: 2, z: 4, core: 2. Of those that a mesh axis runs over, the one named last changes fastest.
Arguments:
- residual: bfloat16 [4096, 2048], P(('grp', 'sp', 'tp')), parts along dimension 0, may hold values from -6 to 6
- grouped_value_heads: bfloat16 [4096, 2, 1024], P(('grp', 'sp'), None, 'tp'), parts along dimension 0, may hold values from -6 to 6
- output_gate_heads: bfloat16 [4096, 2, 1024], P(('grp', 'sp'), None, 'tp'), parts along dimension 0, may hold values from -6 to 6
- projected_key_query: bfloat16 [4096, 384], P(('grp', 'sp')), parts along dimension 0, may hold values from -6 to 6
- raw_step_size: bfloat16 [4096, 2, 16], P(('grp', 'sp'), None, 'tp'), parts along dimension 0, may hold values from -3 to 3
- step_size_bias: float32 [2, 16], P(None, 'tp'), may hold values from -1 to 0.5
- head_decay_logarithm: float32 [2, 16], P(None, 'tp'), may hold values from -16 to -2
- position_extra_decay: float32 [4096], P(('grp', 'sp')), parts along dimension 0, may hold values from -0.7 to 0
- head_skip_weight: float32 [2, 16], P(None, 'tp'), may hold values from 0.5 to 2
- value_kernel_taps: bfloat16 [4, 2, 1024], P(None, None, 'tp'), may hold values from -3 to 3
- key_query_kernel: bfloat16 [4, 384], replicated, may hold values from -3 to 3
- head_norm_gain: float32 [2, 1024], P(None, 'tp'), may hold values from 0.1 to 1.9
- output_matrix: bfloat16 [2, 1024, 2048], P(None, 'tp'), may hold values from -0.125 to 0.125
- expert_norm_gain: float32 [2048], replicated, may hold values from 0.1 to 1.9
- expert_gate_weight: bfloat16 [4, 2048, 4096], P('sp', None, 'tp'), may hold values from -0.125 to 0.125
- expert_up_weight: bfloat16 [4, 2048, 4096], P('sp', None, 'tp'), may hold values from -0.125 to 0.125
- expert_down_weight: bfloat16 [4, 4096, 2048], P('sp', 'tp'), may hold values from -0.09375 to 0.09375
- token_expert_choice: int32 [4096, 2], P(('grp', 'sp', 'tp')), parts along dimension 0, may hold values from 0 to 3, all different within a row; in each aligned block of 128 rows (0 to 127, 128 to 255, ...) at most 65 rows name the same one
- expert_output_weight: float32 [4096, 2], P(('grp', 'sp', 'tp')), parts along dimension 0, may hold values from 0.2 to 1
Outputs:
- layer_out: bfloat16 [4096, 2048], P(('grp', 'sp', 'tp')), parts along dimension 0
There are 2 independent parts, one for each index of `grp`. A program takes and returns all parts, laid end to end along the dimension named above; an argument that names none is the same for every part. Nothing has to cross between parts.
Inputs may be any that keep to these rules, and one draw needn't show every extreme that they name: `token_expert_choice`: each row names two different experts. The token rows of one device name one expert at most 65 times.
All inputs are finite; a program needn't handle non-finite values.
Results may differ from a plain program's by a relative error of at most 0.015.
Values may be sent and summed in bfloat16 or wider, within the bound.
A program may use at most 128 MiB of HBM per device.

v0:
```python
import jax
import jax.numpy as jnp
from jax import lax
from jax.sharding import PartitionSpec as P

HEAD_DIM = 64
STATE_ONE = 64
STATE_TWO = 128
BLOCK = 128


EPSILON = 1e-06


def passed_along(shard, axis, by):
    length = lax.axis_size(axis)
    pairs = [(i, i + by) for i in range(length) if 0 <= i + by < length]
    return lax.ppermute(shard, axis, pairs)


def prefix(shard, axis, join, neutral):
    place = lax.axis_index(axis)
    gathered = jax.tree.map(
        lambda a, kind: lax.all_gather(a.astype(kind), axis),
        shard,
        (jnp.bfloat16, jnp.bfloat16, jnp.bfloat16),
    )
    state = jax.tree.map(lambda a, e: jnp.zeros_like(a) + jnp.asarray(e, a.dtype), shard, neutral)

    def one(step, state):
        return join(
            state,
            jax.tree.map(
                lambda a, own: lax.dynamic_index_in_dim(a, step, 0, False).astype(own.dtype),
                gathered,
                shard,
            ),
        )

    return lax.fori_loop(0, place, one, state)


def causal_taps(extended, tap_weights, length):
    summed = jnp.zeros((length, extended.shape[1]), jnp.float32)
    for offset in range(tap_weights.shape[0]):
        summed = summed + extended[offset : offset + length].astype(jnp.float32) * tap_weights[
            offset
        ].astype(jnp.float32)
    return summed


def advance(carried, pair_item):
    block_state, fading_step = pair_item
    return (carried * fading_step[:, None, None] + block_state, carried)


def local_blocks(value_rows, key_rows, query_rows, step_spacing, decay_logarithm):
    positions, head_count, head_width = value_rows.shape
    block_count = positions // BLOCK
    value_rows = value_rows.reshape(block_count, BLOCK, head_count, head_width)
    key_rows = key_rows.reshape(block_count, BLOCK, key_rows.shape[-1])
    query_rows = query_rows.reshape(block_count, BLOCK, query_rows.shape[-1])
    step_spacing = step_spacing.reshape(block_count, BLOCK, head_count)
    running = jnp.cumsum(decay_logarithm.reshape(block_count, BLOCK, head_count), axis=1)
    scores = jnp.einsum("kln,ksn->kls", query_rows, key_rows, preferred_element_type=jnp.float32)
    causal = jnp.tril(jnp.ones((BLOCK, BLOCK), jnp.bool_))
    spread = running[:, :, None, :] - running[:, None, :, :]
    damping = jnp.exp(jnp.where(causal[None, :, :, None], spread, -jnp.inf))
    weights = (scores[:, :, :, None] * damping * step_spacing[:, None, :, :]).astype(jnp.bfloat16)
    near_part = jnp.einsum(
        "klsh,kshp->klhp", weights, value_rows, preferred_element_type=jnp.float32
    )
    fading = jnp.exp(running[:, -1:, :] - running) * step_spacing
    scaled_keys = (key_rows.astype(jnp.float32)[:, :, None, :] * fading[:, :, :, None]).astype(
        jnp.bfloat16
    )
    states = jnp.einsum(
        "kshn,kshp->khpn", scaled_keys, value_rows, preferred_element_type=jnp.float32
    )
    block_ends = running[:, -1, :]
    anchor = jnp.zeros(states.shape[1:], jnp.float32)
    last_state, entering = lax.scan(advance, anchor, (states, jnp.exp(block_ends)))
    wide_queries = query_rows.astype(jnp.float32)
    far_part = jnp.einsum("kln,khpn->klhp", wide_queries, entering, precision=lax.Precision.HIGHEST)
    far_part = far_part * jnp.exp(running)[:, :, :, None]
    earlier_ends = jnp.cumsum(block_ends, axis=0) - block_ends
    carried_decay = jnp.exp(running + earlier_ends[:, None, :])
    return (
        near_part + far_part,
        last_state,
        jnp.sum(block_ends, axis=0),
        wide_queries,
        carried_decay,
    )


def join_states(earlier, later):
    early_decay, early_one, early_two = earlier
    late_decay, late_one, late_two = later
    return (
        early_decay + late_decay,
        early_one * jnp.exp(late_decay[0])[:, None, None] + late_one,
        early_two * jnp.exp(late_decay[1])[:, None, None] + late_two,
    )


def local(
    residual,
    grouped_value_heads,
    output_gate_heads,
    projected_key_query,
    raw_step_size,
    step_size_bias,
    head_decay_logarithm,
    position_extra_decay,
    head_skip_weight,
    value_kernel_taps,
    key_query_kernel,
    head_norm_gain,
    output_matrix,
    expert_norm_gain,
    expert_gate_weight,
    expert_up_weight,
    expert_down_weight,
    token_expert_choice,
    expert_output_weight,
):
    positions = grouped_value_heads.shape[0]
    lane_width = grouped_value_heads.shape[2]
    local_heads = lane_width // HEAD_DIM
    both_lanes = 2 * lane_width
    rim_depth = key_query_kernel.shape[0] - 1
    flat_values = grouped_value_heads.reshape(positions, both_lanes)
    rim_rows = jnp.concatenate(
        [flat_values[positions - rim_depth :], projected_key_query[positions - rim_depth :]], axis=1
    )
    prior_rows = passed_along(rim_rows, "sp", 1)
    padded_values = jnp.concatenate([prior_rows[:, :both_lanes], flat_values], axis=0)
    padded_keys = jnp.concatenate([prior_rows[:, both_lanes:], projected_key_query], axis=0)
    conv_heads = jax.nn.silu(
        causal_taps(padded_values, value_kernel_taps.reshape(rim_depth + 1, both_lanes), positions)
    ).astype(jnp.bfloat16)
    conv_rows = jax.nn.silu(causal_taps(padded_keys, key_query_kernel, positions)).astype(
        jnp.bfloat16
    )
    step_spacing = jax.nn.softplus(raw_step_size.astype(jnp.float32) + step_size_bias[None])
    decay_logarithm = (
        position_extra_decay[:, None, None] - jnp.exp(head_decay_logarithm)[None] * step_spacing
    )
    value_heads = conv_heads.reshape(positions, 2, local_heads, HEAD_DIM)
    bounds = [0, STATE_ONE, 2 * STATE_ONE, 2 * STATE_ONE + STATE_TWO, 2 * STATE_ONE + 2 * STATE_TWO]
    local_parts = []
    end_states = []
    decay_totals = []
    query_list = []
    reach_list = []
    for group_index in range(2):
        key_rows = conv_rows[:, bounds[2 * group_index] : bounds[2 * group_index + 1]]
        query_rows = conv_rows[:, bounds[2 * group_index + 1] : bounds[2 * group_index + 2]]
        local_part, end_state, decay_total, wide_queries, carried_decay = local_blocks(
            value_heads[:, group_index],
            key_rows,
            query_rows,
            step_spacing[:, group_index],
            decay_logarithm[:, group_index],
        )
        local_parts.append(local_part)
        end_states.append(end_state)
        decay_totals.append(decay_total)
        query_list.append(wide_queries)
        reach_list.append(carried_decay)
    identity = (
        jnp.zeros((2, local_heads), jnp.float32),
        jnp.zeros_like(end_states[0]),
        jnp.zeros_like(end_states[1]),
    )
    prior_decay, enter_one, enter_two = prefix(
        (jnp.stack(decay_totals), end_states[0], end_states[1]), "sp", join_states, identity
    )
    entered = [enter_one, enter_two]
    group_parts = []
    for group_index in range(2):
        carried_part = jnp.einsum(
            "kln,hpn->klhp",
            query_list[group_index],
            entered[group_index],
            precision=lax.Precision.HIGHEST,
        )
        carried_part = carried_part * reach_list[group_index][:, :, :, None]
        summed_part = local_parts[group_index] + carried_part
        group_parts.append(summed_part.reshape(positions, local_heads, HEAD_DIM))
    mixer_sum = jnp.stack(group_parts, axis=1) + head_skip_weight[
        None, :, :, None
    ] * value_heads.astype(jnp.float32)
    gated_rows = mixer_sum * jax.nn.silu(
        output_gate_heads.astype(jnp.float32).reshape(positions, 2, local_heads, HEAD_DIM)
    )
    scale_rows = lax.rsqrt(jnp.mean(gated_rows * gated_rows, axis=3, keepdims=True) + EPSILON)
    mixed_heads = (
        gated_rows * scale_rows * head_norm_gain.reshape(2, local_heads, HEAD_DIM)
    ).astype(jnp.bfloat16)
    mixed_heads = mixed_heads.reshape(positions, 2, lane_width)
    rows_here = residual.shape[0]
    model_width = output_matrix.shape[2]
    mix_out = lax.psum_scatter(
        jnp.einsum(
            "tgc,gcd->td", mixed_heads, output_matrix, preferred_element_type=jnp.float32
        ).astype(jnp.bfloat16),
        "tp",
        scatter_dimension=0,
        tiled=True,
    ).astype(jnp.float32)
    stream = (residual.astype(jnp.float32) + mix_out).astype(jnp.bfloat16)
    wide_stream = stream.astype(jnp.float32)
    normed = (
        wide_stream
        * lax.rsqrt(jnp.mean(wide_stream * wide_stream, axis=1, keepdims=True) + EPSILON)
        * expert_norm_gain[None]
    ).astype(jnp.bfloat16)
    expert_total = lax.axis_size("sp")
    capacity = 2 * rows_here // expert_total + 1
    flat_ids = token_expert_choice.reshape(-1)
    matches = (flat_ids[:, None] == jnp.arange(expert_total, dtype=jnp.int32)[None, :]).astype(
        jnp.int32
    )
    slot_rank = jnp.sum((jnp.cumsum(matches, axis=0) - matches) * matches, axis=1)
    target = flat_ids * capacity + slot_rank
    outbound = (
        jnp.zeros((expert_total * capacity, model_width), jnp.bfloat16)
        .at[target]
        .set(jnp.repeat(normed, 2, axis=0))
    )
    outbound = outbound.reshape(expert_total, capacity, model_width)
    widened = lax.all_gather(
        lax.all_to_all(outbound, "sp", split_axis=0, concat_axis=0, tiled=True),
        "tp",
        axis=0,
        tiled=True,
    )
    flat_rows = widened.reshape(-1, widened.shape[-1])
    gate_out = jnp.dot(flat_rows, expert_gate_weight[0], preferred_element_type=jnp.float32)
    up_out = jnp.dot(flat_rows, expert_up_weight[0], preferred_element_type=jnp.float32)
    hidden = (jax.nn.silu(gate_out) * up_out).astype(jnp.bfloat16)
    partial_value = jnp.dot(
        hidden, expert_down_weight[0], preferred_element_type=jnp.float32
    ).astype(jnp.bfloat16)
    partial_value = lax.optimization_barrier(
        partial_value.reshape(widened.shape[0], widened.shape[1], partial_value.shape[-1])
    ).astype(jnp.float32)
    summed = lax.psum_scatter(
        partial_value.astype(jnp.bfloat16), "tp", scatter_dimension=0, tiled=True
    )
    returned = lax.all_to_all(summed, "sp", split_axis=0, concat_axis=0, tiled=True)
    picked = jnp.take(returned.reshape(expert_total * capacity, model_width), target, axis=0)
    picked = picked.reshape(rows_here, 2, model_width).astype(jnp.float32)
    weighted = (
        expert_output_weight[:, 0:1] * picked[:, 0] + expert_output_weight[:, 1:2] * picked[:, 1]
    )
    return (wide_stream + weighted).astype(jnp.bfloat16)


def solution(mesh):
    placed = (
        P(("grp", "sp", "tp"), None),
        P(("grp", "sp"), None, "tp"),
        P(("grp", "sp"), None, "tp"),
        P(("grp", "sp"), None),
        P(("grp", "sp"), None, "tp"),
        P(None, "tp"),
        P(None, "tp"),
        P(("grp", "sp")),
        P(None, "tp"),
        P(None, None, "tp"),
        P(),
        P(None, "tp"),
        P(None, "tp", None),
        P(),
        P("sp", None, "tp"),
        P("sp", None, "tp"),
        P("sp", "tp", None),
        P(("grp", "sp", "tp"), None),
        P(("grp", "sp", "tp"), None),
    )
    return jax.shard_map(
        local, mesh=mesh, in_specs=placed, out_specs=P(("grp", "sp", "tp"), None), check_vma=False
    )
```

profile of v0, /device:TPU:0, one launch (start us, length us, event | category | flops | bytes accessed | tf_op | source)
XLA Modules:
  0.0 432.2 jit_solution(18423041220971475305)
XLA Ops:
  9.0 3.1 collective-permute-start
  18.9 5.8 %all_gather.19 = bf16[4,2,4]{2,1,0:T(2,128)(2,1)} all-gather(bf16[1,2,4]{2,1,0:T(2,128)(2,1)S(1)} %pad_maximum_fusion.3), channel_id=1, replica_groups=mesh['grp'=2,'sp'=4,'tp'=4] {'sp'}, dimensions={0}, use_global_device_ids=true | all-gather | bytes 80 | tf_op jit(solution)/shard_map/all_gather | solution.py:24
  24.7 2.0 copy.165
  44.8 2.2 multiply_convert_fusion.4
  49.4 3.1 multiply_convert_fusion.3
  56.1 2.3 fusion.33
  58.4 9.2 %while.42 = (s32[]{:T(128)}, f32[4,64,128]{2,1,0:T(8,128)S(1)}, f32[4,4,64,128]{3,2,1,0:T(8,128)}, f32[4,4]{1,0:T(4,128)}, f32[4,4,64,128]{3,2,1,0:T(8,128)}, /*index=5*/s32[]{:T(128)}, s32[]{:T(128)}) while((s32[]{:T(128)}, f32[4,64,128]{2,1,0:T(8,128)S(1)}, f32[4,4,64,128]{3,2,1,0:T(8,128)}, f32[4,4]{1,0:T(4,128)}, ...), condition=%wide.region_7.8_spmd.clone, body=%wide.region_6.7_spmd.clone.sunk | while | flops 131075 | bytes 656016 | solution.py:82
  67.6 6.2 %all-gather.1 = bf16[16,64,128]{2,1,0:T(8,128)(2,1)} all-gather(bf16[4,64,128]{2,1,0:T(8,128)(2,1)S(1)} %convert_element_type.223), channel_id=3, replica_groups=mesh['grp'=2,'sp'=4,'tp'=4] {'sp'}, dimensions={0}, use_global_device_ids=true | all-gather | bytes 327680 | tf_op jit(solution)/shard_map/all_gather | solution.py:24
  73.8 1.7 reshape_squeeze.16
  76.6 2.0 fusion.50
  78.7 9.4 %while.41 = (s32[]{:T(128)}, f32[4,64,64]{2,1,0:T(8,128)S(1)}, f32[4,4,64,64]{3,2,1,0:T(8,128)}, f32[4,4]{1,0:T(4,128)}, f32[4,4,64,64]{3,2,1,0:T(8,128)}, /*index=5*/s32[]{:T(128)}, s32[]{:T(128)}) while((s32[]{:T(128)}, f32[4,64,64]{2,1,0:T(8,128)S(1)}, f32[4,4,64,64]{3,2,1,0:T(8,128)}, f32[4,4]{1,0:T(4,128)}, ...), condition=%wide.region_2.3_spmd.clone, body=%wide.region_1.2_spmd.clone.sunk | while | flops 65539 | bytes 393872 | solution.py:82
  88.1 6.3 %all-gather = bf16[16,64,64]{2,1,0:T(8,128)(2,1)} all-gather(bf16[4,64,64]{2,1,0:T(8,128)(2,1)S(1)} %convert_element_type.220), channel_id=2, replica_groups=mesh['grp'=2,'sp'=4,'tp'=4] {'sp'}, dimensions={0}, use_global_device_ids=true | all-gather | bytes 163840 | tf_op jit(solution)/shard_map/all_gather | solution.py:24
  101.3 2.1 stack_reshape.6
  103.3 2.1 stack.21
  110.1 2.1 stack_reshape.7
  112.2 2.0 stack.22
  117.7 2.6 bitcast_convert_fusion
  122.8 49.9 %reduce-scatter.3.cloned.1.call-done = bf16[128,2048]{1,0:T(8,128)(2,1)} async-done(((bf16[512,2048]{1,0:T(8,128)(2,1)}), bf16[128,2048]{1,0:T(8,128)(2,1)}) %reduce-scatter.3.cloned.1.call-update) | async-done | bytes 524304 | tf_op jit(solution)/shard_map/reduce_scatter | solution.py:205
  176.4 2.4 scatter_custom_fusion
  179.1 19.0 %all_to_all.10 = bf16[4,65,2048]{2,1,0:T(8,128)(2,1)} all-to-all(bf16[4,65,2048]{2,1,0:T(8,128)(2,1)S(1)} %reshape.303), channel_id=1, replica_groups=mesh['grp'=2,'sp'=4,'tp'=4] {'sp'}, dimensions={0} | all-to-all | bytes 2129920 | tf_op jit(solution)/shard_map/all_to_all | solution.py:235
  198.4 87.6 %all-gather.4.cloned.1.call-done = bf16[16,65,2048]{2,1,0:T(8,128)(2,1)} async-done(((bf16[4,65,2048]{2,1,0:T(8,128)(2,1)}), bf16[16,65,2048]{2,1,0:T(8,128)(2,1)}) %all-gather.4.cloned.1.call-update) | async-done | bytes 4259856 | tf_op jit(solution)/shard_map/all_gather | solution.py:234
  285.9 4.4 %reshape.304 = bf16[1040,2048]{1,0:T(8,128)(2,1)} reshape(bf16[16,65,2048]{2,1,0:T(8,128)(2,1)} %all-gather.4.cloned.1.call-done) | data formatting | bytes 8519680 | tf_op jit(solution)/shard_map/reshape | solution.py:240
  290.4 7.7 %fusion.5 = f32[1040,1024]{1,0:T(8,128)S(1)} fusion(bf16[1040,2048]{1,0:T(8,128)(2,1)} %reshape.304, bf16[1,2048,1024]{2,1,0:T(8,128)(2,1)} %param.39), kind=kOutput, calls=%fused_computation.20 | convolution fusion | flops 4362076160 | bytes 12713984 | tf_op jit(solution)/shard_map/dot_general | solution.py:241
  298.2 5.4 %fusion.7 = bf16[1040,1024]{1,0:T(8,128)(2,1)S(1)} fusion(bf16[1040,2048]{1,0:T(8,128)(2,1)S(1)} %copy-done.5, bf16[1,2048,1024]{2,1,0:T(8,128)(2,1)S(1)} %copy-done.14, f32[1040,1024]{1,0:T(8,128)S(1)} %fusion.5), kind=kOutput, calls=%fused_computation.23 | convolution fusion | flops 4368465920 | bytes 14843904 | tf_op jit(solution)/shard_map/dot_general | solution.py:242
  303.5 6.2 %convolution_convert_fusion = bf16[1040,2048]{1,0:T(8,128)(2,1)} fusion(bf16[1040,1024]{1,0:T(8,128)(2,1)S(1)} %fusion.7, bf16[1,1024,2048]{2,1,0:T(8,128)(2,1)S(1)} %copy-done.15), kind=kOutput, calls=%fused_computation.16 | convolution fusion | flops 4364206080 | bytes 10584064 | tf_op jit(solution)/shard_map/dot_general | solution.py:244
  309.7 4.4 %reshape.305 = bf16[16,65,2048]{2,1,0:T(8,128)(2,1)} reshape(bf16[1040,2048]{1,0:T(8,128)(2,1)} %convolution_convert_fusion) | data formatting | bytes 8519680 | tf_op jit(solution)/shard_map/reshape | solution.py:248
  314.1 83.9 %reduce-scatter.5.cloned.1.call-done = bf16[4,65,2048]{2,1,0:T(8,128)(2,1)} async-done(((bf16[16,65,2048]{2,1,0:T(8,128)(2,1)}), bf16[4,65,2048]{2,1,0:T(8,128)(2,1)}) %reduce-scatter.5.cloned.1.call-update) | async-done | bytes 1064976 | tf_op jit(solution)/shard_map/reduce_scatter | solution.py:250
  398.0 3.5 all-to-all-start.1
  401.8 15.5 %all-to-all-done.1 = bf16[4,65,2048]{2,1,0:T(8,128)(2,1)S(1)} async-done(((bf16[4,65,2048]{2,1,0:T(8,128)(2,1)}), bf16[4,65,2048]{2,1,0:T(8,128)(2,1)S(1)}, u32[]{:S(2)}, u32[]{:S(2)}) %all-to-all-start.1) | async-done | bytes 1064992 | tf_op jit(solution)/shard_map/all_to_all | solution.py:253
  417.7 2.3 gather_fusion
  420.0 2.6 gather.7
  422.7 1.9 fusion.28
  (166 shorter events, 75.9 us)
Async XLA Ops:
  6.5 111.2 %copy-start = (bf16[2,256,2048]{2,1,0:T(8,128)(2,1)S(1)}, bf16[2,256,2048]{2,1,0:T(8,128)(2,1)}, u32[]{:S(2)}) copy-start(bf16[2,256,2048]{2,1,0:T(8,128)(2,1)} %param.37) | copy-start | bytes 6291460
  6.5 166.2 %reduce-scatter.3.cloned.1.call-start = ((), (), s32[]{:S(2)}) async-start(), calls=%async_computation.4 | async-start | bytes 2621440 | tf_op jit(solution)/shard_map/reduce_scatter | solution.py:205
  9.0 34.8 %collective-permute-start = (bf16[3,896]{0,1:T(8,128)(2,1)}, bf16[3,896]{0,1:T(8,128)(2,1)}, u32[]{:S(2)}, u32[]{:S(2)}) collective-permute-start(bf16[3,896]{0,1:T(8,128)(2,1)} %copy.164), channel_id=1, source_target_pairs={{0,4},{4,8},{8,12},{1,5},{5,9},{9,13},{2,6},{6,10},{10,14},{3,7},{... | collective-permute-start | bytes 16136 | tf_op jit(solution)/shard_map/ppermute | solution.py:18
  14.2 28.9 %copy-start.10 = (f32[2,4]{1,0:T(2,128)S(1)}, f32[2,4]{1,0:T(2,128)}, u32[]{:S(2)}) copy-start(f32[2,4]{1,0:T(2,128)} %param.33) | copy-start | bytes 100
  95.9 9.5 %copy-start.6 = (bf16[512,128]{1,0:T(8,128)(2,1)S(1)}, bf16[512,128]{1,0:T(8,128)(2,1)}, u32[]{:S(2)}) copy-start(bf16[512,128]{1,0:T(8,128)(2,1)} %get-tuple-element.207) | copy-start | bytes 393220
  105.6 8.6 %copy-start.11 = (f32[2,4]{1,0:T(2,128)S(1)}, f32[2,4]{1,0:T(2,128)}, u32[]{:S(2)}) copy-start(f32[2,4]{1,0:T(2,128)} %param.33) | copy-start | bytes 100
  106.0 9.9 %copy-start.9 = (f32[2,256]{1,0:T(2,128)S(1)}, f32[2,256]{1,0:T(2,128)}, u32[]{:S(2)}) copy-start(f32[2,256]{1,0:T(2,128)} %mul.425) | copy-start | bytes 6148
  106.0 9.9 %copy-start.12 = (f32[2,256]{1,0:T(2,128)S(1)}, f32[2,256]{1,0:T(2,128)}, u32[]{:S(2)}) copy-start(f32[2,256]{1,0:T(2,128)} %param.36) | copy-start | bytes 6148
  117.7 2.7 copy-start.7
  117.7 55.0 %copy-start.2 = (bf16[128,2048]{1,0:T(8,128)(2,1)S(1)}, bf16[128,2048]{1,0:T(8,128)(2,1)}, u32[]{:S(2)}) copy-start(bf16[128,2048]{1,0:T(8,128)(2,1)} %param.25) | copy-start | bytes 1572868
  117.7 56.3 %copy-start.8 = (f32[2048]{0:T(1024)S(1)}, f32[2048]{0:T(1024)}, u32[]{:S(2)}) copy-start(f32[2048]{0:T(1024)} %param.38) | copy-start | bytes 24580
  120.4 165.6 %all-gather.4.cloned.1.call-start = ((), (), s32[]{:S(2)}) async-start(), calls=%async_computation.5 | async-start | bytes 5898240 | tf_op jit(solution)/shard_map/all_gather | solution.py:234
  198.1 199.9 %reduce-scatter.5.cloned.1.call-start = ((), (), s32[]{:S(2)}) async-start(), calls=%async_computation.6 | async-start | bytes 5898240 | tf_op jit(solution)/shard_map/reduce_scatter | solution.py:250
  290.4 7.8 %copy-start.5 = (bf16[1040,2048]{1,0:T(8,128)(2,1)S(1)}, bf16[1040,2048]{1,0:T(8,128)(2,1)}, u32[]{:S(2)}) copy-start(bf16[1040,2048]{1,0:T(8,128)(2,1)} %reshape.304) | copy-start | bytes 12779524
  290.4 7.8 %copy-start.14 = (bf16[1,2048,1024]{2,1,0:T(8,128)(2,1)S(1)}, bf16[1,2048,1024]{2,1,0:T(8,128)(2,1)}, u32[]{:S(2)}) copy-start(bf16[1,2048,1024]{2,1,0:T(8,128)(2,1)} %param.40) | copy-start | bytes 12582916
  298.1 5.4 %copy-start.15 = (bf16[1,1024,2048]{2,1,0:T(8,128)(2,1)S(1)}, bf16[1,1024,2048]{2,1,0:T(8,128)(2,1)}, u32[]{:S(2)}) copy-start(bf16[1,1024,2048]{2,1,0:T(8,128)(2,1)} %param.41) | copy-start | bytes 12582916
  314.1 87.7 %copy-start.13 = (f32[128,2]{0,1:T(2,128)S(1)}, f32[128,2]{0,1:T(2,128)}, u32[]{:S(2)}) copy-start(f32[128,2]{0,1:T(2,128)} %param.43) | copy-start | bytes 3076
  398.0 19.3 %all-to-all-start.1 = ((bf16[4,65,2048]{2,1,0:T(8,128)(2,1)}), bf16[4,65,2048]{2,1,0:T(8,128)(2,1)S(1)}, u32[]{:S(2)}, u32[]{:S(2)}) async-start(bf16[4,65,2048]{2,1,0:T(8,128)(2,1)} %reduce-scatter.5.cloned.1.call-done), calls=%async_computation.3 | async-start | bytes 2359296 | tf_op jit(solution)/shard_map/all_to_all | solution.py:253
  417.7 8.0 %copy-start.1 = (bf16[2,256,2048]{2,1,0:T(8,128)(2,1)S(1)}, bf16[2,256,2048]{2,1,0:T(8,128)(2,1)}, u32[]{:S(2)}) copy-start(bf16[2,256,2048]{2,1,0:T(8,128)(2,1)} %param.37) | copy-start | bytes 6291460
  420.0 4.6 %copy-start.3 = (bf16[128,2048]{1,0:T(8,128)(2,1)S(1)}, bf16[128,2048]{1,0:T(8,128)(2,1)}, u32[]{:S(2)}) copy-start(bf16[128,2048]{1,0:T(8,128)(2,1)} %param.25) | copy-start | bytes 1572868
  420.0 4.6 %copy-start.4 = (bf16[128,2048]{1,0:T(8,128)(2,1)S(1)}, bf16[128,2048]{1,0:T(8,128)(2,1)}, u32[]{:S(2)}) copy-start(bf16[128,2048]{1,0:T(8,128)(2,1)} %reduce-scatter.3.cloned.1.call-done) | copy-start | bytes 1572868
Sparse Core Ops, SparseCore 0:
  120.5 52.1 reduce-scatter.2
  198.2 87.6 all-gather.3
  314.3 83.6 reduce-scatter.4
where the time goes:
time: 434 us; the launch traced here: 432 us
  waiting for transfers between devices  237 us (55%)
  local copies, waits for them, and re-layouts  65.5 us (15%)
  blocking collectives  37.3 us (9%)
  other arithmetic  36.3 us (8%)
  matrix products  35.3 us (8%)
  between operations  13.6 us (3%)
  starting transfers between devices  6.91 us (2%)
    all_gather x1, waiting for transfers between devices, local(): lax.all_gather(lax.all_to_all(outbound, 'sp', split_axis=0, concat_axis=0...  87.6 us
    reduce_scatter x1, waiting for transfers between devices, local(): lax.psum_scatter(partial_value.astype(jnp.bfloat16), 'tp', scatter_dimens...  83.9 us
    reduce_scatter x1, waiting for transfers between devices, local(): lax.psum_scatter(jnp.einsum('tgc,gcd->td', mixed_heads, output_matrix, pr...  49.9 us
    all_to_all x1, blocking collectives, local(): lax.all_to_all(outbound, 'sp', split_axis=0, concat_axis=0, tiled=True)  19 us
    all_gather x3, blocking collectives, prefix(): lax.all_gather(a.astype(kind), axis)  18.3 us
    all_to_all x1, waiting for transfers between devices, local(): lax.all_to_all(summed, 'sp', split_axis=0, concat_axis=0, tiled=True)  15.5 us
  transfers between devices with their start and end apart: 5, of which 4 were waited for; matrix products, arithmetic and copies ran while one was open for 7% of the time, Pallas kernels for 0%

commit v1 on v0

v1 whole, which is shorter than its diff:
```python
import jax
import jax.numpy as jnp
from jax import lax
from jax.experimental import pallas as pl
from jax.experimental.pallas import tpu as pltpu
from jax.sharding import PartitionSpec as P

HEAD_DIM = 64
STATE_ONE = 64
STATE_TWO = 128
BLOCK = 128


EPSILON = 1e-06


def passed_along(shard, axis, by):
    length = lax.axis_size(axis)
    pairs = [(i, i + by) for i in range(length) if 0 <= i + by < length]
    return lax.ppermute(shard, axis, pairs)


HIGHEST = lax.Precision.HIGHEST
PACK_ROWS = 16


def full_dot(left, right):
    return jnp.dot(left, right, precision=HIGHEST, preferred_element_type=jnp.float32)


def spread_matrix(head_count):
    shape = (head_count, head_count * HEAD_DIM)
    rows = lax.broadcasted_iota(jnp.int32, shape, 0)
    lanes = lax.broadcasted_iota(jnp.int32, shape, 1)
    return (lanes // HEAD_DIM == rows).astype(jnp.float32)


def silu(value):
    return value * (1.0 / (1.0 + jnp.exp(-value)))


def state_kernel(
    value_ref, key_ref, prior_ref, raw_ref, bias_ref, rate_ref, extra_ref, value_taps_ref,
    key_taps_ref, conv_ref, conv_key_ref, running_ref, spacing_ref, states_ref, pack_ref, pad_ref,
):
    positions, lanes = value_ref.shape
    taps = value_taps_ref.shape[0]
    half = lanes // 2
    pad_ref[8 - taps + 1 : 8, :] = prior_ref[...].astype(jnp.float32)
    pad_ref[8:, :lanes] = value_ref[...].astype(jnp.float32)
    pad_ref[8:, lanes:] = key_ref[...].astype(jnp.float32)
    spacing = jax.nn.softplus(raw_ref[...].astype(jnp.float32) + bias_ref[...])
    log_decay = extra_ref[...] - jnp.exp(rate_ref[...]) * spacing
    spacing_ref[...] = spacing
    head_count = spacing.shape[1]
    spread = spread_matrix(head_count)
    row = lax.broadcasted_iota(jnp.int32, (BLOCK, BLOCK), 0)
    col = lax.broadcasted_iota(jnp.int32, (BLOCK, BLOCK), 1)
    tril = (row >= col).astype(jnp.float32)
    carried = [jnp.zeros((STATE_ONE, half), jnp.float32), jnp.zeros((STATE_TWO, half), jnp.float32)]
    total = jnp.zeros((1, lanes), jnp.float32)
    starts = (0, 2 * STATE_ONE)
    sizes = (STATE_ONE, STATE_TWO)
    value_taps = value_taps_ref[...].astype(jnp.float32)
    key_taps = key_taps_ref[...].astype(jnp.float32)
    for block in range(positions // BLOCK):
        lo = block * BLOCK
        summed = jnp.zeros((BLOCK, lanes), jnp.float32)
        key_sum = jnp.zeros((BLOCK, key_ref.shape[1]), jnp.float32)
        for tap in range(taps):
            at = lo + 8 - taps + 1 + tap
            summed = summed + pad_ref[at : at + BLOCK, :lanes] * value_taps[tap : tap + 1]
            key_sum = key_sum + pad_ref[at : at + BLOCK, lanes:] * key_taps[tap : tap + 1]
        conv = silu(summed).astype(jnp.bfloat16)
        conv_key = silu(key_sum).astype(jnp.bfloat16)
        conv_ref[lo : lo + BLOCK, :] = conv
        conv_key_ref[lo : lo + BLOCK, :] = conv_key
        running = full_dot(tril, log_decay[lo : lo + BLOCK])
        running_ref[lo : lo + BLOCK, :] = running
        end = running[BLOCK - 1 : BLOCK]
        fading = jnp.exp(end - running) * spacing[lo : lo + BLOCK]
        scaled = (conv.astype(jnp.float32) * full_dot(fading, spread)).astype(jnp.bfloat16)
        wide_end = full_dot(jnp.broadcast_to(end, (8, head_count)), spread)[:1]
        total = total + wide_end
        fade = jnp.exp(wide_end)
        for group in range(2):
            keys = conv_key[:, starts[group] : starts[group] + sizes[group]]
            at = group * STATE_ONE
            states_ref[block, at : at + sizes[group], :] = carried[group]
            state = lax.dot_general(
                keys,
                scaled[:, group * half : (group + 1) * half],
                (((0,), (0,)), ((), ())),
                preferred_element_type=jnp.float32,
            )
            carried[group] = carried[group] * fade[:, group * half : (group + 1) * half] + state
    pack_ref[:STATE_ONE, :] = carried[0].astype(jnp.bfloat16)
    pack_ref[STATE_ONE : STATE_ONE + STATE_TWO, :] = carried[1].astype(jnp.bfloat16)
    high = total.astype(jnp.bfloat16).astype(jnp.float32)
    low = total - high
    line = lax.broadcasted_iota(jnp.int32, (PACK_ROWS, half), 0)
    packed = jnp.zeros((PACK_ROWS, half), jnp.float32)
    for at, piece in enumerate((high[:, :half], high[:, half:], low[:, :half], low[:, half:])):
        packed = jnp.where(line == at, piece, packed)
    pack_ref[STATE_ONE + STATE_TWO :, :] = packed.astype(jnp.bfloat16)


def mix_kernel(
    place_ref, conv_ref, key_ref, running_ref, spacing_ref, states_ref, packs_ref, gate_ref,
    skip_ref, gain_ref, matrix_ref, out_ref, entered_ref, reach_ref,
):
    block = pl.program_id(0)
    lanes = conv_ref.shape[1]
    half = lanes // 2
    depth = STATE_ONE + STATE_TWO
    head_count = spacing_ref.shape[1]
    spread = spread_matrix(head_count)

    @pl.when(block == 0)
    def _():
        reach_ref[...] = jnp.zeros_like(reach_ref)
        entered_ref[...] = jnp.zeros_like(entered_ref)
        for source in range(packs_ref.shape[0] - 1):

            @pl.when(source < place_ref[0])
            def _():
                decay = packs_ref[source, depth:, :].astype(jnp.float32)
                one = jnp.exp(decay[0:1] + decay[2:3])
                two = jnp.exp(decay[1:2] + decay[3:4])
                entered_ref[:STATE_ONE, :] = entered_ref[:STATE_ONE, :] * one + packs_ref[
                    source, :STATE_ONE, :
                ].astype(jnp.float32)
                entered_ref[STATE_ONE:, :] = entered_ref[STATE_ONE:, :] * two + packs_ref[
                    source, STATE_ONE:depth, :
                ].astype(jnp.float32)

    running = running_ref[...]
    spacing = spacing_ref[...]
    running_rows = running.T
    spacing_rows = spacing.T
    wide_running = full_dot(running, spread)
    reach = reach_ref[0:1, :]
    reach_fade = jnp.exp(reach)
    reach_ref[0:1, :] = reach + wide_running[BLOCK - 1 : BLOCK]
    wide_fade = jnp.exp(wide_running)
    row = lax.broadcasted_iota(jnp.int32, (BLOCK, BLOCK), 0)
    col = lax.broadcasted_iota(jnp.int32, (BLOCK, BLOCK), 1)
    causal = row >= col
    low_lanes = lax.broadcasted_iota(jnp.int32, (BLOCK, 2 * HEAD_DIM), 1) < HEAD_DIM
    starts = (0, 2 * STATE_ONE)
    sizes = (STATE_ONE, STATE_TWO)
    pair_lanes = 2 * HEAD_DIM
    mean_shape = (pair_lanes, pair_lanes)
    mean_rows = lax.broadcasted_iota(jnp.int32, mean_shape, 0) // HEAD_DIM
    mean_cols = lax.broadcasted_iota(jnp.int32, mean_shape, 1) // HEAD_DIM
    averaging = jnp.where(mean_rows == mean_cols, 1.0 / HEAD_DIM, 0.0)
    mixed = []
    for group in range(2):
        at = starts[group]
        size = sizes[group]
        keys = key_ref[:, at : at + size]
        queries = key_ref[:, at + size : at + 2 * size]
        scores = lax.dot_general(
            queries, keys, (((1,), (1,)), ((), ())), preferred_element_type=jnp.float32
        )
        rows = slice(group * STATE_ONE, group * STATE_ONE + size)
        cols = slice(group * half, (group + 1) * half)
        entering = states_ref[0, rows, :] + entered_ref[rows, :] * reach_fade[:, cols]
        far = jnp.dot(queries, entering.astype(jnp.bfloat16), preferred_element_type=jnp.float32)
        far = far * wide_fade[:, cols]
        for pair in range(half // pair_lanes):
            lane = group * half + pair * pair_lanes
            here = slice(lane, lane + pair_lanes)
            values = conv_ref[:, here]
            zero = jnp.zeros_like(values)
            stacked = jnp.concatenate(
                [jnp.where(low_lanes, values, zero), jnp.where(low_lanes, zero, values)], axis=0
            )
            weights = []
            for head in (lane // HEAD_DIM, lane // HEAD_DIM + 1):
                gap = running[:, head : head + 1] - running_rows[head : head + 1, :]
                damping = jnp.exp(jnp.where(causal, gap, -jnp.inf))
                weights.append(
                    (scores * damping * spacing_rows[head : head + 1, :]).astype(jnp.bfloat16)
                )
            near = jnp.dot(
                jnp.concatenate(weights, axis=1), stacked, preferred_element_type=jnp.float32
            )
            summed = near + far[:, pair * pair_lanes : (pair + 1) * pair_lanes]
            summed = summed + skip_ref[:, here] * values.astype(jnp.float32)
            gated = summed * silu(gate_ref[:, here].astype(jnp.float32))
            scale = lax.rsqrt(full_dot(gated * gated, averaging) + EPSILON)
            mixed.append((gated * scale * gain_ref[:, here]).astype(jnp.bfloat16))
    mixed = jnp.concatenate(mixed, axis=1)
    out_ref[...] = jnp.dot(mixed, matrix_ref[...], preferred_element_type=jnp.float32).astype(
        jnp.bfloat16
    )


def mixer(
    values, gates, key_query, prior_rows, raw, bias, rate, extra, skip, value_taps, key_taps, gain,
    matrix,
):
    positions, lanes = values.shape
    key_width = key_query.shape[1]
    heads = raw.shape[1]
    half = lanes // 2
    blocks = positions // BLOCK
    depth = STATE_ONE + STATE_TWO
    model_width = matrix.shape[1]
    vmem = pl.BlockSpec(memory_space=pltpu.VMEM)
    conv, conv_key, running, spacing, states, pack = pl.pallas_call(
        state_kernel,
        out_shape=(
            jax.ShapeDtypeStruct((positions, lanes), jnp.bfloat16),
            jax.ShapeDtypeStruct((positions, key_width), jnp.bfloat16),
            jax.ShapeDtypeStruct((positions, heads), jnp.float32),
            jax.ShapeDtypeStruct((positions, heads), jnp.float32),
            jax.ShapeDtypeStruct((blocks, depth, half), jnp.float32),
            jax.ShapeDtypeStruct((depth + PACK_ROWS, half), jnp.bfloat16),
        ),
        in_specs=[vmem] * 9,
        out_specs=[vmem] * 6,
        scratch_shapes=[pltpu.VMEM((8 + positions, lanes + key_width), jnp.float32)],
        compiler_params=pltpu.CompilerParams(vmem_limit_bytes=32 * 1024 * 1024),
        name="mixer_states",
    )(values, key_query, prior_rows, raw, bias, rate, extra, value_taps, key_taps)
    packs = lax.all_gather(pack, "sp")
    place = lax.axis_index("sp").astype(jnp.int32).reshape(1)

    def by_block(width):
        return pl.BlockSpec((BLOCK, width), lambda k: (k, 0))

    def whole(*shape):
        return pl.BlockSpec(shape, lambda k: (0,) * len(shape))

    return pl.pallas_call(
        mix_kernel,
        grid=(blocks,),
        out_shape=jax.ShapeDtypeStruct((positions, model_width), jnp.bfloat16),
        in_specs=[
            pl.BlockSpec(memory_space=pltpu.SMEM),
            by_block(lanes),
            by_block(key_width),
            by_block(heads),
            by_block(heads),
            pl.BlockSpec((1, depth, half), lambda k: (k, 0, 0)),
            whole(*packs.shape),
            by_block(lanes),
            whole(1, lanes),
            whole(1, lanes),
            whole(lanes, model_width),
        ],
        out_specs=by_block(model_width),
        scratch_shapes=[pltpu.VMEM((depth, half), jnp.float32), pltpu.VMEM((8, lanes), jnp.float32)],
        compiler_params=pltpu.CompilerParams(vmem_limit_bytes=32 * 1024 * 1024),
        name="mixer_output",
    )(place, conv, conv_key, running, spacing, states, packs, gates, skip, gain, matrix)


def local(
    residual,
    grouped_value_heads,
    output_gate_heads,
    projected_key_query,
    raw_step_size,
    step_size_bias,
    head_decay_logarithm,
    position_extra_decay,
    head_skip_weight,
    value_kernel_taps,
    key_query_kernel,
    head_norm_gain,
    output_matrix,
    expert_norm_gain,
    expert_gate_weight,
    expert_up_weight,
    expert_down_weight,
    token_expert_choice,
    expert_output_weight,
):
    positions = grouped_value_heads.shape[0]
    lane_width = grouped_value_heads.shape[2]
    local_heads = lane_width // HEAD_DIM
    both_lanes = 2 * lane_width
    rim_depth = key_query_kernel.shape[0] - 1
    flat_values = grouped_value_heads.reshape(positions, both_lanes)
    rim_rows = jnp.concatenate(
        [flat_values[positions - rim_depth :], projected_key_query[positions - rim_depth :]], axis=1
    )
    prior_rows = passed_along(rim_rows, "sp", 1)
    both_heads = 2 * local_heads
    mix_partial = mixer(
        flat_values,
        output_gate_heads.reshape(positions, both_lanes),
        projected_key_query,
        prior_rows,
        raw_step_size.reshape(positions, both_heads),
        step_size_bias.reshape(1, both_heads),
        head_decay_logarithm.reshape(1, both_heads),
        position_extra_decay.reshape(positions, 1),
        jnp.repeat(head_skip_weight.reshape(1, both_heads), HEAD_DIM, axis=1),
        value_kernel_taps.reshape(rim_depth + 1, both_lanes),
        key_query_kernel,
        head_norm_gain.reshape(1, both_lanes),
        output_matrix.reshape(both_lanes, output_matrix.shape[2]),
    )
    rows_here = residual.shape[0]
    model_width = output_matrix.shape[2]
    mix_out = lax.psum_scatter(mix_partial, "tp", scatter_dimension=0, tiled=True).astype(jnp.float32)
    stream = (residual.astype(jnp.float32) + mix_out).astype(jnp.bfloat16)
    wide_stream = stream.astype(jnp.float32)
    normed = (
        wide_stream
        * lax.rsqrt(jnp.mean(wide_stream * wide_stream, axis=1, keepdims=True) + EPSILON)
        * expert_norm_gain[None]
    ).astype(jnp.bfloat16)
    expert_total = lax.axis_size("sp")
    capacity = 2 * rows_here // expert_total + 1
    flat_ids = token_expert_choice.reshape(-1)
    matches = (flat_ids[:, None] == jnp.arange(expert_total, dtype=jnp.int32)[None, :]).astype(
        jnp.int32
    )
    slot_rank = jnp.sum((jnp.cumsum(matches, axis=0) - matches) * matches, axis=1)
    target = flat_ids * capacity + slot_rank
    outbound = (
        jnp.zeros((expert_total * capacity, model_width), jnp.bfloat16)
        .at[target]
        .set(jnp.repeat(normed, 2, axis=0))
    )
    outbound = outbound.reshape(expert_total, capacity, model_width)
    widened = lax.all_gather(
        lax.all_to_all(outbound, "sp", split_axis=0, concat_axis=0, tiled=True),
        "tp",
        axis=0,
        tiled=True,
    )
    flat_rows = widened.reshape(-1, widened.shape[-1])
    gate_out = jnp.dot(flat_rows, expert_gate_weight[0], preferred_element_type=jnp.float32)
    up_out = jnp.dot(flat_rows, expert_up_weight[0], preferred_element_type=jnp.float32)
    hidden = (jax.nn.silu(gate_out) * up_out).astype(jnp.bfloat16)
    partial_value = jnp.dot(
        hidden, expert_down_weight[0], preferred_element_type=jnp.float32
    ).astype(jnp.bfloat16)
    partial_value = lax.optimization_barrier(
        partial_value.reshape(widened.shape[0], widened.shape[1], partial_value.shape[-1])
    ).astype(jnp.float32)
    summed = lax.psum_scatter(
        partial_value.astype(jnp.bfloat16), "tp", scatter_dimension=0, tiled=True
    )
    returned = lax.all_to_all(summed, "sp", split_axis=0, concat_axis=0, tiled=True)
    picked = jnp.take(returned.reshape(expert_total * capacity, model_width), target, axis=0)
    picked = picked.reshape(rows_here, 2, model_width).astype(jnp.float32)
    weighted = (
        expert_output_weight[:, 0:1] * picked[:, 0] + expert_output_weight[:, 1:2] * picked[:, 1]
    )
    return (wide_stream + weighted).astype(jnp.bfloat16)


def solution(mesh):
    placed = (
        P(("grp", "sp", "tp"), None),
        P(("grp", "sp"), None, "tp"),
        P(("grp", "sp"), None, "tp"),
        P(("grp", "sp"), None),
        P(("grp", "sp"), None, "tp"),
        P(None, "tp"),
        P(None, "tp"),
        P(("grp", "sp")),
        P(None, "tp"),
        P(None, None, "tp"),
        P(),
        P(None, "tp"),
        P(None, "tp", None),
        P(),
        P("sp", None, "tp"),
        P("sp", None, "tp"),
        P("sp", "tp", None),
        P(("grp", "sp", "tp"), None),
        P(("grp", "sp", "tp"), None),
    )
    return jax.shard_map(
        local, mesh=mesh, in_specs=placed, out_specs=P(("grp", "sp", "tp"), None), check_vma=False
    )
```

time: 434 us -> 345 us (0.79)
  local copies, waits for them, and re-layouts: 65.5 us -> 30.9 us
  other arithmetic: 36.3 us -> 6.66 us
  matrix products: 35.3 us -> 19.3 us
  Pallas kernels: 0 us -> 11.3 us
  blocking collectives: 37.3 us -> 26.5 us
  waiting for transfers between devices: 237 us -> 230 us
    dot_general x11 -> x0, matrix products: 16 us -> none  [the longest x2 4.32 us: local_blocks(): jnp.einsum('kshn,kshp->khpn', scaled_keys, value_rows, preferred_element_...]
    another operation x17 -> x2, local copies, waits for them, and re-layouts: 14.4 us -> 0.1 us  [the longest x4 8.23 us: local(): jnp.stack(group_parts, axis=1)]
    pallas_call x0 -> x2, Pallas kernels: none -> 11.3 us  [the longest x1 7.41 us: mixer(): pl.pallas_call(mix_kernel, grid=(blocks,), out_shape=jax.ShapeDtypeStruct...]
    all_gather x3 -> x1, blocking collectives: 18.3 us -> 7.55 us  [mixer(): packs = lax.all_gather(pack, 'sp')]
    mul x13 -> x0, local copies, waits for them, and re-layouts: 10 us -> none  [the longest x8 5.25 us: advance(): return (carried * fading_step[:, None, None] + block_state, carried)]
    convert_element_type x6 -> x0, other arithmetic: 8.03 us -> none  [the longest x1 3.15 us: local(): conv_heads = jax.nn.silu(causal_taps(padded_values, value_kernel_taps.res...]
    add x8 -> x0, other arithmetic: 7.88 us -> none  [advance(): return (carried * fading_step[:, None, None] + block_state, carried)]
    exp x7 -> x0, local copies, waits for them, and re-layouts: 7.26 us -> none  [the longest x2 2.73 us: local_blocks(): far_part = far_part * jnp.exp(running)[:, :, :, None]]
  transfers between devices with their start and end apart: 5 -> 5, of which waited for: 4 -> 4; matrix products, arithmetic and copies ran while one was open for 7% -> 4% of each run, Pallas kernels for 0% -> 0%
where the time goes in v1:
time: 345 us; the launch traced here: 344 us
  waiting for transfers between devices  230 us (67%)
  local copies, waits for them, and re-layouts  30.9 us (9%)
  blocking collectives  26.5 us (8%)
  matrix products  19.3 us (6%)
  between operations  13.4 us (4%)
  Pallas kernels  11.3 us (3%)
  other arithmetic  6.66 us (2%)
  starting transfers between devices  6.18 us (2%)
    all_gather x1, waiting for transfers between devices, local(): lax.all_gather(lax.all_to_all(outbound, 'sp', split_axis=0, concat_axis=0...  87.6 us
    reduce_scatter x1, waiting for transfers between devices, local(): lax.psum_scatter(partial_value.astype(jnp.bfloat16), 'tp', scatter_dimens...  83.9 us
    reduce_scatter x1, waiting for transfers between devices, local(): lax.psum_scatter(mix_partial, 'tp', scatter_dimension=0, tiled=True)  43 us
    all_to_all x1, blocking collectives, local(): lax.all_to_all(outbound, 'sp', split_axis=0, concat_axis=0, tiled=True)  19 us
    all_to_all x1, waiting for transfers between devices, local(): lax.all_to_all(summed, 'sp', split_axis=0, concat_axis=0, tiled=True)  15.5 us
    dot_general x1, matrix products, local(): jnp.dot(flat_rows, expert_gate_weight[0], preferred_element_type=jnp.floa...  7.74 us
    unnamed x33, local copies, waits for them, and re-layouts  7.64 us
    all_gather x1, blocking collectives, mixer(): packs = lax.all_gather(pack, 'sp')  7.55 us
  transfers between devices with their start and end apart: 5, of which 4 were waited for; matrix products, arithmetic and copies ran while one was open for 4% of the time, Pallas kernels for 0%

profile of v1, /device:TPU:0, one launch (start us, length us, event | category | flops | bytes accessed | tf_op | source)
XLA Modules:
  0.0 344.3 jit_solution(7795991265930950629)
XLA Ops:
  6.5 0.8 slice_bitcast_fusion.2
  8.7 2.4 collective-permute-start
  11.1 1.1 copy.50
  12.2 0.8 copy.42.extra_ref
  13.0 0.7 reshape.128
  14.6 1.3 reshape.129.bias_ref
  16.0 1.3 reshape.130.rate_ref
  17.3 1.1 copy.53
  18.4 0.8 reshape.134
  19.8 0.7 broadcast_in_dim.26.skip_ref
  21.3 1.0 copy-done.1
  24.3 3.9 %mixer_states.1 = (bf16[512,512]{1,0:T(8,128)(2,1)S(1)}, bf16[512,384]{1,0:T(8,128)(2,1)S(1)}, f32[512,8]{1,0:T(8,128)S(1)}, f32[512,8]{1,0:T(8,128)S(1)}, f32[4...) custom-call(bf16[512,512]{1,0:T(8,128)(2,1)S(1)} %bitcast.73, bf16[512,384]{1,0:T(8,128)(2,1)S(1)} %copy-done.1, ...), custom_call_target="tpu_custom_call" | custom-call | tf_op jit(solution)/shard_map/mixer_states/pallas_call | solution.py:212
  28.1 7.5 %all-gather = bf16[832,256]{1,0:T(8,128)(2,1)S(1)} all-gather(bf16[208,256]{1,0:T(8,128)(2,1)S(1)} %get-tuple-element.16), channel_id=2, replica_groups=mesh['grp'=2,'sp'=4,'tp'=4] {'sp'}, dimensions={0}, use_global_device_ids=true | all-gather | bytes 532480 | tf_op jit(solution)/shard_map/all_gather | solution.py:228
  35.7 7.4 %mixer_output.1 = bf16[512,2048]{1,0:T(8,128)(2,1)} custom-call(s32[1]{0:T(128)} %bitcast.place_ref, bf16[512,512]{1,0:T(8,128)(2,1)S(1)} %get-tuple-element.11.conv_ref, bf16[512,384]{1,0:T(8,128)(2,1)S(1)} %get-tuple-element.12.key_ref, f32[512,8]{1,0:T(8,128)S(1)} %get-tuple-element.13.running_ref, f32[512,8]{1,0:T(8,128)S(1)} %get-tuple-element.14.spacing_ref, ...), custom_call_target="tpu_custom_call" | custom-call | tf_op jit(solution)/shard_map/mixer_output/pallas_call | solution.py:237
  43.6 1.2 reduce-window.6
  45.5 43.0 %reduce-scatter.3.cloned.1.call-done = bf16[128,2048]{1,0:T(8,128)(2,1)} async-done(((bf16[512,2048]{1,0:T(8,128)(2,1)}), bf16[128,2048]{1,0:T(8,128)(2,1)}) %reduce-scatter.3.cloned.1.call-update) | async-done | bytes 524304 | tf_op jit(solution)/shard_map/reduce_scatter | solution.py:310
  88.5 1.5 fusion.7
  90.0 1.4 fusion.9
  92.5 2.4 scatter_custom_fusion
  95.2 19.0 %all_to_all.10 = bf16[4,65,2048]{2,1,0:T(8,128)(2,1)} all-to-all(bf16[4,65,2048]{2,1,0:T(8,128)(2,1)S(1)} %reshape.140), channel_id=1, replica_groups=mesh['grp'=2,'sp'=4,'tp'=4] {'sp'}, dimensions={0} | all-to-all | bytes 2129920 | tf_op jit(solution)/shard_map/all_to_all | solution.py:333
  114.5 87.6 %all-gather.3.cloned.1.call-done = bf16[16,65,2048]{2,1,0:T(8,128)(2,1)} async-done(((bf16[4,65,2048]{2,1,0:T(8,128)(2,1)}), bf16[16,65,2048]{2,1,0:T(8,128)(2,1)}) %all-gather.3.cloned.1.call-update) | async-done | bytes 4259856 | tf_op jit(solution)/shard_map/all_gather | solution.py:332
  202.1 4.5 %reshape.141 = bf16[1040,2048]{1,0:T(8,128)(2,1)} reshape(bf16[16,65,2048]{2,1,0:T(8,128)(2,1)} %all-gather.3.cloned.1.call-done) | data formatting | bytes 8519680 | tf_op jit(solution)/shard_map/reshape | solution.py:338
  206.5 7.7 %fusion.2 = f32[1040,1024]{1,0:T(8,128)S(1)} fusion(bf16[1040,2048]{1,0:T(8,128)(2,1)} %reshape.141, bf16[1,2048,1024]{2,1,0:T(8,128)(2,1)} %param.33), kind=kOutput, calls=%fused_computation.6 | convolution fusion | flops 4362076160 | bytes 12713984 | tf_op jit(solution)/shard_map/dot_general | solution.py:339
  214.3 5.4 %fusion.4 = bf16[1040,1024]{1,0:T(8,128)(2,1)S(1)} fusion(bf16[1040,2048]{1,0:T(8,128)(2,1)S(1)} %copy-done.7, bf16[1,2048,1024]{2,1,0:T(8,128)(2,1)S(1)} %copy-done.11, f32[1040,1024]{1,0:T(8,128)S(1)} %fusion.2), kind=kOutput, calls=%fused_computation.8 | convolution fusion | flops 4368465920 | bytes 14843904 | tf_op jit(solution)/shard_map/dot_general | solution.py:340
  219.7 6.2 %convolution_convert_fusion = bf16[1040,2048]{1,0:T(8,128)(2,1)} fusion(bf16[1040,1024]{1,0:T(8,128)(2,1)S(1)} %fusion.4, bf16[1,1024,2048]{2,1,0:T(8,128)(2,1)S(1)} %copy-done.12), kind=kOutput, calls=%fused_computation.2 | convolution fusion | flops 4364206080 | bytes 10584064 | tf_op jit(solution)/shard_map/dot_general | solution.py:342
  225.9 4.4 %reshape.142 = bf16[16,65,2048]{2,1,0:T(8,128)(2,1)} reshape(bf16[1040,2048]{1,0:T(8,128)(2,1)} %convolution_convert_fusion) | data formatting | bytes 8519680 | tf_op jit(solution)/shard_map/reshape | solution.py:346
  230.3 83.9 %reduce-scatter.5.cloned.1.call-done = bf16[4,65,2048]{2,1,0:T(8,128)(2,1)} async-done(((bf16[16,65,2048]{2,1,0:T(8,128)(2,1)}), bf16[4,65,2048]{2,1,0:T(8,128)(2,1)}) %reduce-scatter.5.cloned.1.call-update) | async-done | bytes 1064976 | tf_op jit(solution)/shard_map/reduce_scatter | solution.py:348
  314.2 3.5 %all-to-all-start.1 = ((bf16[4,65,2048]{2,1,0:T(8,128)(2,1)}), bf16[4,65,2048]{2,1,0:T(8,128)(2,1)S(1)}, u32[]{:S(2)}, u32[]{:S(2)}) async-start(bf16[4,65,2048]{2,1,0:T(8,128)(2,1)} %reduce-scatter.5.cloned.1.call-done), calls=%async_computation.3 | async-start | bytes 2359296 | tf_op jit(solution)/shard_map/all_to_all | solution.py:351
  318.0 15.5 %all-to-all-done.1 = bf16[4,65,2048]{2,1,0:T(8,128)(2,1)S(1)} async-done(((bf16[4,65,2048]{2,1,0:T(8,128)(2,1)}), bf16[4,65,2048]{2,1,0:T(8,128)(2,1)S(1)}, u32[]{:S(2)}, u32[]{:S(2)}) %all-to-all-start.1) | async-done | bytes 1064992 | tf_op jit(solution)/shard_map/all_to_all | solution.py:351
  333.8 1.4 gather_fusion
  335.2 0.7 gather.7
  336.7 1.1 fusion.10
  (65 shorter events, 9.5 us)
Async XLA Ops:
  6.5 29.1 %copy-start = (bf16[2,256,2048]{2,1,0:T(8,128)(2,1)S(1)}, bf16[2,256,2048]{2,1,0:T(8,128)(2,1)}, u32[]{:S(2)}) copy-start(bf16[2,256,2048]{2,1,0:T(8,128)(2,1)} %param.31) | copy-start | bytes 6291460
  6.5 82.0 %reduce-scatter.3.cloned.1.call-start = ((), (), s32[]{:S(2)}) async-start(), calls=%async_computation.4 | async-start | bytes 2621440 | tf_op jit(solution)/shard_map/reduce_scatter | solution.py:310
  8.7 12.6 %collective-permute-start = (bf16[3,896]{1,0:T(4,128)(2,1)}, bf16[3,896]{1,0:T(4,128)(2,1)S(1)}, u32[]{:S(2)}, u32[]{:S(2)}) collective-permute-start(bf16[3,896]{1,0:T(4,128)(2,1)} %pad_maximum_fusion), channel_id=1, source_target_pairs={{0,4},{4,8},{8,12},{1,5},{5,9},{9,13},{2,6},{6,10},{10,14},{3,7},{... | collective-permute-start | bytes 16136 | tf_op jit(solution)/shard_map/ppermute | solution.py:20
  21.3 1.0 copy-start.1
  22.3 0.7 copy-start.2
  22.9 0.7 copy-start.3
  23.6 0.7 copy-start.4
  35.7 7.5 %copy-start.8 = (s32[128,2]{0,1:T(2,128)S(1)}, s32[128,2]{0,1:T(2,128)}, u32[]{:S(2)}) copy-start(s32[128,2]{0,1:T(2,128)} %param.36) | copy-start | bytes 3076
  35.7 54.3 %copy-start.9 = (f32[2048]{0:T(1024)S(1)}, f32[2048]{0:T(1024)}, u32[]{:S(2)}) copy-start(f32[2048]{0:T(1024)} %param.32) | copy-start | bytes 24580
  43.1 159.0 %all-gather.3.cloned.1.call-start = ((), (), s32[]{:S(2)}) async-start(), calls=%async_computation.5 | async-start | bytes 5898240 | tf_op jit(solution)/shard_map/all_gather | solution.py:332
  114.2 200.0 %reduce-scatter.5.cloned.1.call-start = ((), (), s32[]{:S(2)}) async-start(), calls=%async_computation.6 | async-start | bytes 5898240 | tf_op jit(solution)/shard_map/reduce_scatter | solution.py:348
  206.5 7.7 %copy-start.7 = (bf16[1040,2048]{1,0:T(8,128)(2,1)S(1)}, bf16[1040,2048]{1,0:T(8,128)(2,1)}, u32[]{:S(2)}) copy-start(bf16[1040,2048]{1,0:T(8,128)(2,1)} %reshape.141) | copy-start | bytes 12779524
  206.5 7.8 %copy-start.11 = (bf16[1,2048,1024]{2,1,0:T(8,128)(2,1)S(1)}, bf16[1,2048,1024]{2,1,0:T(8,128)(2,1)}, u32[]{:S(2)}) copy-start(bf16[1,2048,1024]{2,1,0:T(8,128)(2,1)} %param.34) | copy-start | bytes 12582916
  214.3 5.4 %copy-start.12 = (bf16[1,1024,2048]{2,1,0:T(8,128)(2,1)S(1)}, bf16[1,1024,2048]{2,1,0:T(8,128)(2,1)}, u32[]{:S(2)}) copy-start(bf16[1,1024,2048]{2,1,0:T(8,128)(2,1)} %param.35) | copy-start | bytes 12582916
  230.3 87.7 %copy-start.10 = (f32[128,2]{0,1:T(2,128)S(1)}, f32[128,2]{0,1:T(2,128)}, u32[]{:S(2)}) copy-start(f32[128,2]{0,1:T(2,128)} %param.37) | copy-start | bytes 3076
  314.2 19.3 %all-to-all-start.1 = ((bf16[4,65,2048]{2,1,0:T(8,128)(2,1)}), bf16[4,65,2048]{2,1,0:T(8,128)(2,1)S(1)}, u32[]{:S(2)}, u32[]{:S(2)}) async-start(bf16[4,65,2048]{2,1,0:T(8,128)(2,1)} %reduce-scatter.5.cloned.1.call-done), calls=%async_computation.3 | async-start | bytes 2359296 | tf_op jit(solution)/shard_map/all_to_all | solution.py:351
  335.2 1.4 copy-start.5
  335.2 1.4 copy-start.6
Sparse Core Ops, SparseCore 0:
  43.2 45.2 reduce-scatter.2
  114.4 87.6 all-gather.2
  230.5 83.6 reduce-scatter.4

commit v2 on v1

--- a/solution.py
+++ b/solution.py
@@ -316,7 +316,8 @@
         * expert_norm_gain[None]
     ).astype(jnp.bfloat16)
     expert_total = lax.axis_size("sp")
-    capacity = 2 * rows_here // expert_total + 1
+    capacity = -(-(2 * rows_here // expert_total + 1) // 8) * 8
+    first_rows = capacity // 16 * 8
     flat_ids = token_expert_choice.reshape(-1)
     matches = (flat_ids[:, None] == jnp.arange(expert_total, dtype=jnp.int32)[None, :]).astype(
         jnp.int32
@@ -329,26 +330,29 @@
         .set(jnp.repeat(normed, 2, axis=0))
     )
     outbound = outbound.reshape(expert_total, capacity, model_width)
-    widened = lax.all_gather(
-        lax.all_to_all(outbound, "sp", split_axis=0, concat_axis=0, tiled=True),
-        "tp",
-        axis=0,
-        tiled=True,
-    )
-    flat_rows = widened.reshape(-1, widened.shape[-1])
-    gate_out = jnp.dot(flat_rows, expert_gate_weight[0], preferred_element_type=jnp.float32)
-    up_out = jnp.dot(flat_rows, expert_up_weight[0], preferred_element_type=jnp.float32)
-    hidden = (jax.nn.silu(gate_out) * up_out).astype(jnp.bfloat16)
-    partial_value = jnp.dot(
-        hidden, expert_down_weight[0], preferred_element_type=jnp.float32
-    ).astype(jnp.bfloat16)
-    partial_value = lax.optimization_barrier(
-        partial_value.reshape(widened.shape[0], widened.shape[1], partial_value.shape[-1])
-    ).astype(jnp.float32)
-    summed = lax.psum_scatter(
-        partial_value.astype(jnp.bfloat16), "tp", scatter_dimension=0, tiled=True
-    )
-    returned = lax.all_to_all(summed, "sp", split_axis=0, concat_axis=0, tiled=True)
+    sent = [
+        lax.all_to_all(piece, "sp", split_axis=0, concat_axis=0, tiled=True)
+        for piece in (outbound[:, :first_rows], outbound[:, first_rows:])
+    ]
+    widened = [lax.all_gather(piece, "tp", axis=0, tiled=True) for piece in sent]
+    summed = []
+    for piece in widened:
+        flat_rows = piece.reshape(-1, model_width)
+        gate_out = jnp.dot(flat_rows, expert_gate_weight[0], preferred_element_type=jnp.float32)
+        up_out = jnp.dot(flat_rows, expert_up_weight[0], preferred_element_type=jnp.float32)
+        hidden = (jax.nn.silu(gate_out) * up_out).astype(jnp.bfloat16)
+        partial_value = jnp.dot(
+            hidden, expert_down_weight[0], preferred_element_type=jnp.float32
+        ).astype(jnp.bfloat16)
+        summed.append(
+            lax.psum_scatter(
+                partial_value.reshape(piece.shape), "tp", scatter_dimension=0, tiled=True
+            )
+        )
+    returned = jnp.concatenate(
+        [lax.all_to_all(piece, "sp", split_axis=0, concat_axis=0, tiled=True) for piece in summed],
+        axis=1,
+    )
     picked = jnp.take(returned.reshape(expert_total * capacity, model_width), target, axis=0)
     picked = picked.reshape(rows_here, 2, model_width).astype(jnp.float32)
     weighted = (

time: 345 us -> 331 us (0.959)
  waiting for transfers between devices: 230 us -> 187 us
  blocking collectives: 26.5 us -> 45 us
  matrix products: 19.3 us -> 36.8 us
  local copies, waits for them, and re-layouts: 30.9 us -> 22.2 us
    all_gather x1 -> x2, waiting for transfers between devices: 87.6 us -> 68.3 us  [local(): lax.all_gather(piece, 'tp', axis=0, tiled=True)]
    all_to_all x1 -> x3, blocking collectives: 19 us -> 37.5 us  [local(): lax.all_to_all(piece, 'sp', split_axis=0, concat_axis=0, tiled=True)]
    reduce_scatter x1 -> x2, waiting for transfers between devices: 83.9 us -> 66.3 us  [local(): lax.psum_scatter(partial_value.reshape(piece.shape), 'tp', scatter_dimens...]
    dot_general x1 -> x2, matrix products: 6.22 us -> 22.8 us  [local(): jnp.dot(hidden, expert_down_weight[0], preferred_element_type=jnp.float32)]
    reshape x4 -> x0, local copies, waits for them, and re-layouts: 9.45 us -> none  [the longest x1 4.46 us: local(): flat_rows = widened.reshape(-1, widened.shape[-1])]
    all_to_all x1, waiting for transfers between devices: 15.5 us -> 9.71 us  [local(): lax.all_to_all(piece, 'sp', split_axis=0, concat_axis=0, tiled=True)]
    unnamed x33 -> x29, local copies, waits for them, and re-layouts: 7.64 us -> 7.57 us
  transfers between devices with their start and end apart: 5 -> 7, of which waited for: 4 -> 6; matrix products, arithmetic and copies ran while one was open for 4% -> 15% of each run, Pallas kernels for 0% -> 0%
where the time goes in v2:
time: 331 us; the launch traced here: 330 us
  waiting for transfers between devices  187 us (56%)
  blocking collectives  45 us (14%)
  matrix products  36.8 us (11%)
  local copies, waits for them, and re-layouts  22.2 us (7%)
  between operations  13.4 us (4%)
  Pallas kernels  11.3 us (3%)
  other arithmetic  7.69 us (2%)
  starting transfers between devices  6.44 us (2%)
    all_gather x2, waiting for transfers between devices, local(): lax.all_gather(piece, 'tp', axis=0, tiled=True)  68.3 us
    reduce_scatter x2, waiting for transfers between devices, local(): lax.psum_scatter(partial_value.reshape(piece.shape), 'tp', scatter_dimens...  66.3 us
    reduce_scatter x1, waiting for transfers between devices, local(): lax.psum_scatter(mix_partial, 'tp', scatter_dimension=0, tiled=True)  43 us
    all_to_all x3, blocking collectives, local(): lax.all_to_all(piece, 'sp', split_axis=0, concat_axis=0, tiled=True)  37.5 us
    dot_general x2, matrix products, local(): jnp.dot(hidden, expert_down_weight[0], preferred_element_type=jnp.float32)  22.8 us
    all_to_all x1, waiting for transfers between devices, local(): lax.all_to_all(piece, 'sp', split_axis=0, concat_axis=0, tiled=True)  9.71 us
    unnamed x29, local copies, waits for them, and re-layouts  7.57 us
    all_gather x1, blocking collectives, mixer(): packs = lax.all_gather(pack, 'sp')  7.53 us
  transfers between devices with their start and end apart: 7, of which 6 were waited for; matrix products, arithmetic and copies ran while one was open for 15% of the time, Pallas kernels for 0%

profile of v2, /device:TPU:0, one launch (start us, length us, event | category | flops | bytes accessed | tf_op | source)
XLA Modules:
  0.0 330.2 jit_solution(12382729868780777918)
XLA Ops:
  6.5 0.8 slice_bitcast_fusion.2
  8.7 2.4 collective-permute-start
  11.1 1.1 copy.50
  14.6 1.3 reshape.135.bias_ref
  15.9 1.3 reshape.136.rate_ref
  17.2 1.1 copy.53
  21.2 1.0 copy-done.1
  24.2 3.9 %mixer_states.1 = (bf16[512,512]{1,0:T(8,128)(2,1)S(1)}, bf16[512,384]{1,0:T(8,128)(2,1)S(1)}, f32[512,8]{1,0:T(8,128)S(1)}, f32[512,8]{1,0:T(8,128)S(1)}, f32[4...) custom-call(bf16[512,512]{1,0:T(8,128)(2,1)S(1)} %bitcast.96, bf16[512,384]{1,0:T(8,128)(2,1)S(1)} %copy-done.1, ...), custom_call_target="tpu_custom_call" | custom-call | tf_op jit(solution)/shard_map/mixer_states/pallas_call | solution.py:212
  28.1 7.5 %all-gather = bf16[832,256]{1,0:T(8,128)(2,1)S(1)} all-gather(bf16[208,256]{1,0:T(8,128)(2,1)S(1)} %get-tuple-element.16), channel_id=2, replica_groups=mesh['grp'=2,'sp'=4,'tp'=4] {'sp'}, dimensions={0}, use_global_device_ids=true | all-gather | bytes 532480 | tf_op jit(solution)/shard_map/all_gather | solution.py:228
  35.6 7.4 %mixer_output.1 = bf16[512,2048]{1,0:T(8,128)(2,1)} custom-call(s32[1]{0:T(128)} %bitcast.place_ref, bf16[512,512]{1,0:T(8,128)(2,1)S(1)} %get-tuple-element.11.conv_ref, bf16[512,384]{1,0:T(8,128)(2,1)S(1)} %get-tuple-element.12.key_ref, f32[512,8]{1,0:T(8,128)S(1)} %get-tuple-element.13.running_ref, f32[512,8]{1,0:T(8,128)S(1)} %get-tuple-element.14.spacing_ref, ...), custom_call_target="tpu_custom_call" | custom-call | tf_op jit(solution)/shard_map/mixer_output/pallas_call | solution.py:237
  43.5 1.2 reduce-window.6
  45.4 43.0 %reduce-scatter.4.cloned.1.call-done = bf16[128,2048]{1,0:T(8,128)(2,1)} async-done(((bf16[512,2048]{1,0:T(8,128)(2,1)}), bf16[128,2048]{1,0:T(8,128)(2,1)}) %reduce-scatter.4.cloned.1.call-update) | async-done | bytes 524304 | tf_op jit(solution)/shard_map/reduce_scatter | solution.py:310
  88.4 1.3 fusion.22
  89.7 1.3 fusion.24
  92.1 2.5 scatter_custom_fusion
  94.6 11.9 %all_to_all.20 = bf16[4,32,2048]{2,1,0:T(8,128)(2,1)} all-to-all(bf16[4,32,2048]{2,1,0:T(8,128)(2,1)S(1)} %slice.47), channel_id=1, replica_groups=mesh['grp'=2,'sp'=4,'tp'=4] {'sp'}, dimensions={0} | all-to-all | bytes 1048576 | tf_op jit(solution)/shard_map/all_to_all | solution.py:334
  106.6 13.3 %all_to_all.21 = bf16[4,40,2048]{2,1,0:T(8,128)(2,1)} all-to-all(bf16[4,40,2048]{2,1,0:T(8,128)(2,1)S(1)} %slice.48), channel_id=1, replica_groups=mesh['grp'=2,'sp'=4,'tp'=4] {'sp'}, dimensions={0} | all-to-all | bytes 1310720 | tf_op jit(solution)/shard_map/all_to_all | solution.py:334
  120.2 30.4 %all-gather.4.cloned.1.call-done = bf16[16,32,2048]{2,1,0:T(8,128)(2,1)} async-done(((bf16[4,32,2048]{2,1,0:T(8,128)(2,1)}), bf16[16,32,2048]{2,1,0:T(8,128)(2,1)}) %all-gather.4.cloned.1.call-update) | async-done | bytes 2097168 | tf_op jit(solution)/shard_map/all_gather | solution.py:337
  150.6 6.7 %fusion.10 = f32[512,1024]{1,0:T(8,128)} fusion(bf16[512,2048]{1,0:T(8,128)(2,1)} %bitcast.117, bf16[1,2048,1024]{2,1,0:T(8,128)(2,1)} %param.33), kind=kOutput, calls=%fused_computation.12 | convolution fusion | flops 2147483648 | bytes 8388608 | tf_op jit(solution)/shard_map/dot_general | solution.py:341
  157.3 10.5 %fusion.15 = bf16[512,2048]{1,0:T(8,128)(2,1)} fusion(bf16[1,1024,2048]{2,1,0:T(8,128)(2,1)} %param.35, f32[512,1024]{1,0:T(8,128)} %fusion.10, bf16[512,2048]{1,0:T(8,128)(2,1)S(1)} %bitcast.118, bf16[1,2048,1024]{2,1,0:T(8,128)(2,1)} %param.34), kind=kOutput, calls=%fused_computation.15 | convolution fusion | flops 4299161600 | bytes 14680064 | tf_op jit(solution)/shard_map/dot_general | solution.py:344
  167.9 37.9 %all-gather.6.cloned.1.call-done = bf16[16,40,2048]{2,1,0:T(8,128)(2,1)} async-done(((bf16[4,40,2048]{2,1,0:T(8,128)(2,1)}), bf16[16,40,2048]{2,1,0:T(8,128)(2,1)}) %all-gather.6.cloned.1.call-update) | async-done | bytes 2621456 | tf_op jit(solution)/shard_map/all_gather | solution.py:337
  205.8 7.3 %fusion.4 = f32[640,1024]{1,0:T(8,128)} fusion(bf16[640,2048]{1,0:T(8,128)(2,1)} %bitcast.115, bf16[1,2048,1024]{2,1,0:T(8,128)(2,1)} %param.34), kind=kOutput, calls=%fused_computation.6 | convolution fusion | flops 2684354560 | bytes 9437184 | tf_op jit(solution)/shard_map/dot_general | solution.py:342
  213.1 12.3 %fusion.12 = bf16[640,2048]{1,0:T(8,128)(2,1)} fusion(bf16[1,1024,2048]{2,1,0:T(8,128)(2,1)} %param.35, f32[640,1024]{1,0:T(8,128)} %fusion.4, bf16[640,2048]{1,0:T(8,128)(2,1)} %bitcast.116, bf16[1,2048,1024]{2,1,0:T(8,128)(2,1)} %param.33), kind=kOutput, calls=%fused_computation.14 | convolution fusion | flops 5373952000 | bytes 16252928 | tf_op jit(solution)/shard_map/dot_general | solution.py:344
  225.5 24.9 %reduce-scatter.6.cloned.1.call-done = bf16[4,32,2048]{2,1,0:T(8,128)(2,1)} async-done(((bf16[16,32,2048]{2,1,0:T(8,128)(2,1)}), bf16[4,32,2048]{2,1,0:T(8,128)(2,1)}) %reduce-scatter.6.cloned.1.call-update) | async-done | bytes 524304 | tf_op jit(solution)/shard_map/reduce_scatter | solution.py:348
  250.4 12.3 %all_to_all.22 = bf16[4,32,2048]{2,1,0:T(8,128)(2,1)S(1)} all-to-all(bf16[4,32,2048]{2,1,0:T(8,128)(2,1)} %reduce-scatter.6.cloned.1.call-done), channel_id=1, replica_groups=mesh['grp'=2,'sp'=4,'tp'=4] {'sp'}, dimensions={0} | all-to-all | bytes 1048576 | tf_op jit(solution)/shard_map/all_to_all | solution.py:353
  262.6 41.4 %reduce-scatter.8.cloned.1.call-done = bf16[4,40,2048]{2,1,0:T(8,128)(2,1)} async-done(((bf16[16,40,2048]{2,1,0:T(8,128)(2,1)}), bf16[4,40,2048]{2,1,0:T(8,128)(2,1)}) %reduce-scatter.8.cloned.1.call-update) | async-done | bytes 655376 | tf_op jit(solution)/shard_map/reduce_scatter | solution.py:348
  304.0 3.7 %all-to-all-start.3 = ((bf16[4,40,2048]{2,1,0:T(8,128)(2,1)}), bf16[4,40,2048]{2,1,0:T(8,128)(2,1)S(1)}, u32[]{:S(2)}, u32[]{:S(2)}) async-start(bf16[4,40,2048]{2,1,0:T(8,128)(2,1)} %reduce-scatter.8.cloned.1.call-done), calls=%async_computation.6 | async-start | bytes 1310720 | tf_op jit(solution)/shard_map/all_to_all | solution.py:353
  308.0 9.7 %all-to-all-done.3 = bf16[4,40,2048]{2,1,0:T(8,128)(2,1)S(1)} async-done(((bf16[4,40,2048]{2,1,0:T(8,128)(2,1)}), bf16[4,40,2048]{2,1,0:T(8,128)(2,1)S(1)}, u32[]{:S(2)}, u32[]{:S(2)}) %all-to-all-start.3) | async-done | bytes 655392 | tf_op jit(solution)/shard_map/all_to_all | solution.py:353
  317.8 1.4 gather_fusion
  319.2 1.5 gather.7
  320.7 1.9 fusion.29
  322.6 1.1 fusion.25
  (69 shorter events, 11.6 us)
Async XLA Ops:
  6.5 29.1 %copy-start = (bf16[2,256,2048]{2,1,0:T(8,128)(2,1)S(1)}, bf16[2,256,2048]{2,1,0:T(8,128)(2,1)}, u32[]{:S(2)}) copy-start(bf16[2,256,2048]{2,1,0:T(8,128)(2,1)} %param.31) | copy-start | bytes 6291460
  6.5 81.9 %reduce-scatter.4.cloned.1.call-start = ((), (), s32[]{:S(2)}) async-start(), calls=%async_computation.7 | async-start | bytes 2621440 | tf_op jit(solution)/shard_map/reduce_scatter | solution.py:310
  8.7 12.6 %collective-permute-start = (bf16[3,896]{1,0:T(4,128)(2,1)}, bf16[3,896]{1,0:T(4,128)(2,1)S(1)}, u32[]{:S(2)}, u32[]{:S(2)}) collective-permute-start(bf16[3,896]{1,0:T(4,128)(2,1)} %pad_maximum_fusion.1), channel_id=1, source_target_pairs={{0,4},{4,8},{8,12},{1,5},{5,9},{9,13},{2,6},{6,10},{10,14},{3,7},{... | collective-permute-start | bytes 16136 | tf_op jit(solution)/shard_map/ppermute | solution.py:20
  21.2 1.0 copy-start.1
  22.2 0.7 copy-start.2
  22.9 0.7 copy-start.3
  23.6 0.6 copy-start.4
  35.6 7.5 %copy-start.7 = (s32[128,2]{0,1:T(2,128)S(1)}, s32[128,2]{0,1:T(2,128)}, u32[]{:S(2)}) copy-start(s32[128,2]{0,1:T(2,128)} %param.36) | copy-start | bytes 3076
  43.0 45.4 %copy-start.5 = (bf16[128,2048]{1,0:T(8,128)(2,1)S(1)}, bf16[128,2048]{1,0:T(8,128)(2,1)}, u32[]{:S(2)}) copy-start(bf16[128,2048]{1,0:T(8,128)(2,1)} %param.19) | copy-start | bytes 1572868
  43.0 46.7 %copy-start.8 = (f32[2048]{0:T(1024)S(1)}, f32[2048]{0:T(1024)}, u32[]{:S(2)}) copy-start(f32[2048]{0:T(1024)} %param.32) | copy-start | bytes 24580
  43.0 107.6 %all-gather.4.cloned.1.call-start = ((), (), s32[]{:S(2)}) async-start(), calls=%async_computation.8 | async-start | bytes 2621440 | tf_op jit(solution)/shard_map/all_gather | solution.py:337
  106.5 99.3 %all-gather.6.cloned.1.call-start = ((), (), s32[]{:S(2)}) async-start(), calls=%async_computation.10 | async-start | bytes 3276800 | tf_op jit(solution)/shard_map/all_gather | solution.py:337
  120.0 130.4 %reduce-scatter.6.cloned.1.call-start = ((), (), s32[]{:S(2)}) async-start(), calls=%async_computation.9 | async-start | bytes 2621440 | tf_op jit(solution)/shard_map/reduce_scatter | solution.py:348
  150.6 6.7 %copy-start.10 = (bf16[16,32,2048]{2,1,0:T(8,128)(2,1)S(1)}, bf16[16,32,2048]{2,1,0:T(8,128)(2,1)}, u32[]{:S(2)}) copy-start(bf16[16,32,2048]{2,1,0:T(8,128)(2,1)} %all-gather.4.cloned.1.call-done) | copy-start | bytes 6291460
  167.8 136.2 %reduce-scatter.8.cloned.1.call-start = ((), (), s32[]{:S(2)}) async-start(), calls=%async_computation.11 | async-start | bytes 3276800 | tf_op jit(solution)/shard_map/reduce_scatter | solution.py:348
  225.4 82.5 %copy-start.9 = (f32[128,2]{0,1:T(2,128)S(1)}, f32[128,2]{0,1:T(2,128)}, u32[]{:S(2)}) copy-start(f32[128,2]{0,1:T(2,128)} %param.37) | copy-start | bytes 3076
  304.0 13.7 %all-to-all-start.3 = ((bf16[4,40,2048]{2,1,0:T(8,128)(2,1)}), bf16[4,40,2048]{2,1,0:T(8,128)(2,1)S(1)}, u32[]{:S(2)}, u32[]{:S(2)}) async-start(bf16[4,40,2048]{2,1,0:T(8,128)(2,1)} %reduce-scatter.8.cloned.1.call-done), calls=%async_computation.6 | async-start | bytes 1310720 | tf_op jit(solution)/shard_map/all_to_all | solution.py:353
  319.2 3.4 %copy-start.6 = (bf16[128,2048]{1,0:T(8,128)(2,1)S(1)}, bf16[128,2048]{1,0:T(8,128)(2,1)}, u32[]{:S(2)}) copy-start(bf16[128,2048]{1,0:T(8,128)(2,1)} %reduce-scatter.4.cloned.1.call-done) | copy-start | bytes 1572868
Sparse Core Ops, SparseCore 0:
  43.1 45.2 reduce-scatter.3
  106.6 43.9 all-gather.3
  152.2 53.5 all-gather.5
  207.9 42.3 reduce-scatter.5
  252.5 51.4 reduce-scatter.7
